TPU v7x, 128 devices: a whole 4x4x4 slice. The times are simulated.
128 devices in a mesh: rep: 2 (over x_hi), fs: 16 (over y, x_lo, core), tp: 4 (over z).
Axes of the slice: x: 4 (x_hi: 2, x_lo: 2; x = x_hi * 2 + x_lo), y: 4, z: 4, core: 2. Of those that a mesh axis runs over, the one named last changes fastest.
Arguments:
- tokens: bfloat16 [16384, 2048], P(('rep', 'fs', 'tp')), may hold values from -3 to 3
- mixer_output: bfloat16 [16384, 2048], P(('rep', 'fs', 'tp')), may hold values from -6 to 6
- early_norm: float32 [2048], replicated, may hold values from 0.75 to 1.25
- early_gate: bfloat16 [2048, 5120], P('fs', 'tp'), may hold values from -0.125 to 0.125
- early_value: bfloat16 [2048, 5120], P('fs', 'tp'), may hold values from -0.125 to 0.125
- early_down: bfloat16 [5120, 2048], P('tp', 'fs'), may hold values from -0.078125 to 0.078125
- early_post: float32 [2048], replicated, may hold values from 0.75 to 1.25
- mixer_gain: float32 [2048], replicated, may hold values from 0.75 to 1.25
- later_norm: float32 [2048], replicated, may hold values from 0.75 to 1.25
- later_gate: bfloat16 [2048, 5120], P('fs', 'tp'), may hold values from -0.125 to 0.125
- later_value: bfloat16 [2048, 5120], P('fs', 'tp'), may hold values from -0.125 to 0.125
- later_down: bfloat16 [5120, 2048], P('tp', 'fs'), may hold values from -0.078125 to 0.078125
- later_post: float32 [2048], replicated, may hold values from 0.75 to 1.25
Outputs:
- layer_out: bfloat16 [16384, 2048], P(('rep', 'fs', 'tp'))
All inputs are finite; a program needn't handle non-finite values.
Results may differ from a plain program's by a relative error of at most 0.015.
Values may be sent and summed in bfloat16 or wider, within the bound.
A program may use at most 128 MiB of HBM per device.

v0:
```python
import jax
import jax.numpy as jnp
from jax import lax
from jax.sharding import PartitionSpec as P

epsilon = 1e-06


def over_all(piece, axis, dim, step, start):

    def gathered(part):
        return lax.all_gather(part, axis, axis=dim, tiled=True)

    return step(start, jax.tree.map(gathered, piece), jnp.int32(0))


def own_rows(product, extent, axis):
    everything = product(jnp.int32(0), lax.axis_size(axis) * extent)
    own = lax.psum_scatter(everything.astype(jnp.bfloat16), axis, scatter_dimension=0, tiled=True)
    return own.astype(jnp.float32)


def rms_scale(values, gain):
    values = values.astype(jnp.float32)
    scale = lax.rsqrt(jnp.mean(values * values, axis=-1, keepdims=True) + epsilon)
    return values * scale * gain


def half_branch(normed, gate_piece, value_piece, down_piece):
    all_rows = lax.all_gather(normed, "tp", axis=0, tiled=True)
    empty = jnp.zeros((all_rows.shape[0], gate_piece.shape[1]), jnp.float32)

    def add_rows(totals, pieces, start):
        columns = lax.dynamic_slice_in_dim(all_rows, start, pieces[0].shape[0], 1)
        gate_part = jnp.dot(columns, pieces[0], preferred_element_type=jnp.float32)
        value_part = jnp.dot(columns, pieces[1], preferred_element_type=jnp.float32)
        return (totals[0] + gate_part, totals[1] + value_part)

    gate_sum, value_sum = over_all((gate_piece, value_piece), "fs", 0, add_rows, (empty, empty))
    down_block = lax.all_gather(down_piece, "fs", axis=1, tiled=True)
    hidden = (jax.nn.silu(gate_sum) * value_sum).astype(jnp.bfloat16)

    def row_term(start, count):
        rows = lax.dynamic_slice_in_dim(hidden, start, count, 0)
        return jnp.dot(rows, down_block, preferred_element_type=jnp.float32)

    return own_rows(row_term, normed.shape[0], "tp")


def on_device(
    tokens,
    mixer_output,
    early_norm,
    early_gate,
    early_value,
    early_down,
    early_post,
    mixer_gain,
    later_norm,
    later_gate,
    later_value,
    later_down,
    later_post,
):
    early_in = rms_scale(tokens, early_norm).astype(jnp.bfloat16)
    early_branch = half_branch(early_in, early_gate, early_value, early_down)
    mixed = (
        tokens.astype(jnp.float32)
        + 0.5 * rms_scale(early_branch, early_post)
        + rms_scale(mixer_output, mixer_gain)
    )
    mixed = mixed.astype(jnp.bfloat16)
    later_in = rms_scale(mixed, later_norm).astype(jnp.bfloat16)
    later_branch = half_branch(later_in, later_gate, later_value, later_down)
    layer_out = mixed.astype(jnp.float32) + 0.5 * rms_scale(later_branch, later_post)
    return layer_out.astype(jnp.bfloat16)


def solution(mesh):
    placed = (
        P(("rep", "fs", "tp"), None),
        P(("rep", "fs", "tp"), None),
        P(),
        P("fs", "tp"),
        P("fs", "tp"),
        P("tp", "fs"),
        P(),
        P(),
        P(),
        P("fs", "tp"),
        P("fs", "tp"),
        P("tp", "fs"),
        P(),
    )
    return jax.shard_map(
        on_device,
        mesh=mesh,
        in_specs=placed,
        out_specs=P(("rep", "fs", "tp"), None),
        check_vma=False,
    )
```

profile of v0, /device:TPU:1, one launch (start us, length us, event | category | flops | bytes accessed | tf_op | source)
XLA Modules:
  0.0 438.2 jit_solution(11551723246681318497)
XLA Ops:
  6.5 1.2 fusion.12
  7.8 2.0 fusion.14
  9.9 0.7 all-gather.11.cloned.1.call-update
  10.6 0.7 all-gather.13.cloned.1.call-update
  11.9 32.1 %all-gather.9.cloned.1.call-done = bf16[512,2048]{1,0:T(8,128)(2,1)} async-done(((bf16[128,2048]{1,0:T(8,128)(2,1)}), bf16[512,2048]{1,0:T(8,128)(2,1)}) %all-gather.9.cloned.1.call-update) | async-done | bytes 2097168 | tf_op jit(solution)/shard_map/all_gather | solution.py:30
  44.0 41.1 %all-gather.11.cloned.1.call-done = bf16[2048,1280]{1,0:T(8,128)(2,1)} async-done(((bf16[128,1280]{1,0:T(8,128)(2,1)}), bf16[2048,1280]{1,0:T(8,128)(2,1)}) %all-gather.11.cloned.1.call-update) | async-done | bytes 5242896 | tf_op jit(solution)/shard_map/all_gather | solution.py:12
  85.1 7.5 %fusion.22 = f32[512,1280]{1,0:T(8,128)} fusion(bf16[512,2048]{1,0:T(8,128)(2,1)} %all-gather.9.cloned.1.call-done, bf16[2048,1280]{1,0:T(8,128)(2,1)} %all-gather.11.cloned.1.call-done), kind=kOutput, calls=%fused_computation.42 | convolution fusion | flops 2684354560 | bytes 9961472 | tf_op jit(solution)/shard_map/dot_general | solution.py:35
  92.6 33.7 %all-gather.13.cloned.1.call-done = bf16[2048,1280]{1,0:T(8,128)(2,1)} async-done(((bf16[128,1280]{1,0:T(8,128)(2,1)}), bf16[2048,1280]{1,0:T(8,128)(2,1)}) %all-gather.13.cloned.1.call-update) | async-done | bytes 5242896 | tf_op jit(solution)/shard_map/all_gather | solution.py:12
  126.3 51.5 %all-gather.15.cloned.1.call-done = bf16[1280,2048]{1,0:T(8,128)(2,1)} async-done(((bf16[1280,128]{1,0:T(8,128)(2,1)}), bf16[1280,2048]{1,0:T(8,128)(2,1)}) %all-gather.15.cloned.1.call-update) | async-done | bytes 5242896 | tf_op jit(solution)/shard_map/all_gather | solution.py:40
  177.8 12.5 %convolution_convert_fusion.1 = bf16[512,2048]{1,0:T(8,128)(2,1)} fusion(bf16[1280,2048]{1,0:T(8,128)(2,1)} %all-gather.15.cloned.1.call-done, bf16[512,2048]{1,0:T(8,128)(2,1)S(1)} %copy-done.6, bf16[2048,1280]{1,0:T(8,128)(2,1)} %all-gather.13.cloned.1.call-done, f32[512,1280]{1,0:T(8,128)} %fusion.22), kind=kOutput, calls=%fused_computation.5 | convolution fusion | flops 5373689856 | bytes 17301504 | tf_op jit(solution)/shard_map/dot_general | solution.py:45
  191.5 28.4 %reduce-scatter.3.cloned.1.call-done = bf16[128,2048]{1,0:T(8,128)(2,1)} async-done(((bf16[512,2048]{1,0:T(8,128)(2,1)}), bf16[128,2048]{1,0:T(8,128)(2,1)}) %reduce-scatter.3.cloned.1.call-update) | async-done | bytes 524304 | tf_op jit(solution)/shard_map/reduce_scatter | solution.py:19
  219.9 1.2 fusion.2
  221.2 1.6 fusion.15
  222.8 1.0 fusion.17
  223.9 0.7 all-gather.21.cloned.1.call-update
  225.6 34.9 %all-gather.19.cloned.1.call-done = bf16[2048,1280]{1,0:T(8,128)(2,1)} async-done(((bf16[128,1280]{1,0:T(8,128)(2,1)}), bf16[2048,1280]{1,0:T(8,128)(2,1)}) %all-gather.19.cloned.1.call-update) | async-done | bytes 5242896 | tf_op jit(solution)/shard_map/all_gather | solution.py:12
  260.5 32.6 %all-gather.17.cloned.1.call-done = bf16[512,2048]{1,0:T(8,128)(2,1)} async-done(((bf16[128,2048]{1,0:T(8,128)(2,1)}), bf16[512,2048]{1,0:T(8,128)(2,1)}) %all-gather.17.cloned.1.call-update) | async-done | bytes 2097168 | tf_op jit(solution)/shard_map/all_gather | solution.py:30
  293.1 7.6 %fusion.23 = f32[512,1280]{1,0:T(8,128)} fusion(bf16[512,2048]{1,0:T(8,128)(2,1)} %all-gather.17.cloned.1.call-done, bf16[2048,1280]{1,0:T(8,128)(2,1)} %all-gather.19.cloned.1.call-done), kind=kOutput, calls=%fused_computation.43 | convolution fusion | flops 2684354560 | bytes 9961472 | tf_op jit(solution)/shard_map/dot_general | solution.py:35
  300.8 33.5 %all-gather.21.cloned.1.call-done = bf16[2048,1280]{1,0:T(8,128)(2,1)} async-done(((bf16[128,1280]{1,0:T(8,128)(2,1)}), bf16[2048,1280]{1,0:T(8,128)(2,1)}) %all-gather.21.cloned.1.call-update) | async-done | bytes 5242896 | tf_op jit(solution)/shard_map/all_gather | solution.py:12
  334.2 51.6 %all-gather.23.cloned.1.call-done = bf16[1280,2048]{1,0:T(8,128)(2,1)} async-done(((bf16[1280,128]{1,0:T(8,128)(2,1)}), bf16[1280,2048]{1,0:T(8,128)(2,1)}) %all-gather.23.cloned.1.call-update) | async-done | bytes 5242896 | tf_op jit(solution)/shard_map/all_gather | solution.py:40
  385.9 12.5 %convolution_convert_fusion = bf16[512,2048]{1,0:T(8,128)(2,1)} fusion(bf16[1280,2048]{1,0:T(8,128)(2,1)} %all-gather.23.cloned.1.call-done, bf16[512,2048]{1,0:T(8,128)(2,1)S(1)} %copy-done.7, bf16[2048,1280]{1,0:T(8,128)(2,1)} %all-gather.21.cloned.1.call-done, f32[512,1280]{1,0:T(8,128)} %fusion.23), kind=kOutput, calls=%fused_computation.4 | convolution fusion | flops 5373689856 | bytes 17301504 | tf_op jit(solution)/shard_map/dot_general | solution.py:45
  398.4 29.6 %reduce-scatter.5.cloned.1.call-done = bf16[128,2048]{1,0:T(8,128)(2,1)} async-done(((bf16[512,2048]{1,0:T(8,128)(2,1)}), bf16[128,2048]{1,0:T(8,128)(2,1)}) %reduce-scatter.5.cloned.1.call-update) | async-done | bytes 524304 | tf_op jit(solution)/shard_map/reduce_scatter | solution.py:19
  428.0 1.2 fusion.9
  429.2 2.1 fusion.18
  (39 shorter events, 3.0 us)
Async XLA Ops:
  6.5 37.5 %all-gather.9.cloned.1.call-start = ((), (), s32[]{:S(2)}) async-start(), calls=%async_computation.2 | async-start | bytes 2621440 | tf_op jit(solution)/shard_map/all_gather | solution.py:30
  9.8 75.3 %all-gather.11.cloned.1.call-start = ((), (), s32[]{:S(2)}) async-start(), calls=%async_computation.3 | async-start | bytes 5570560 | tf_op jit(solution)/shard_map/all_gather | solution.py:12
  10.6 115.7 %all-gather.13.cloned.1.call-start = ((), (), s32[]{:S(2)}) async-start(), calls=%async_computation.4 | async-start | bytes 5570560 | tf_op jit(solution)/shard_map/all_gather | solution.py:12
  11.3 166.5 %all-gather.15.cloned.1.call-start = ((), (), s32[]{:S(2)}) async-start(), calls=%async_computation.5 | async-start | bytes 5570560 | tf_op jit(solution)/shard_map/all_gather | solution.py:40
  11.9 208.0 %reduce-scatter.3.cloned.1.call-start = ((), (), s32[]{:S(2)}) async-start(), calls=%async_computation.6 | async-start | bytes 2621440 | tf_op jit(solution)/shard_map/reduce_scatter | solution.py:19
  44.0 133.8 %copy-start.6 = (bf16[512,2048]{1,0:T(8,128)(2,1)S(1)}, bf16[512,2048]{1,0:T(8,128)(2,1)}, u32[]{:S(2)}) copy-start(bf16[512,2048]{1,0:T(8,128)(2,1)} %all-gather.9.cloned.1.call-done) | copy-start | bytes 6291460
  190.3 1.0 copy-start.1
  190.3 30.9 %copy-start = (bf16[128,2048]{1,0:T(8,128)(2,1)S(1)}, bf16[128,2048]{1,0:T(8,128)(2,1)}, u32[]{:S(2)}) copy-start(bf16[128,2048]{1,0:T(8,128)(2,1)} %param.13) | copy-start | bytes 1572868
  190.3 30.9 %copy-start.2 = (f32[2048]{0:T(1024)S(1)}, f32[2048]{0:T(1024)}, u32[]{:S(2)}) copy-start(f32[2048]{0:T(1024)} %param.20) | copy-start | bytes 24580
  190.3 30.9 %copy-start.3 = (f32[2048]{0:T(1024)S(1)}, f32[2048]{0:T(1024)}, u32[]{:S(2)}) copy-start(f32[2048]{0:T(1024)} %param.19) | copy-start | bytes 24580
  190.3 32.6 %copy-start.4 = (f32[2048]{0:T(1024)S(1)}, f32[2048]{0:T(1024)}, u32[]{:S(2)}) copy-start(f32[2048]{0:T(1024)} %param.21) | copy-start | bytes 24580
  190.3 70.2 %all-gather.19.cloned.1.call-start = ((), (), s32[]{:S(2)}) async-start(), calls=%async_computation.8 | async-start | bytes 5570560 | tf_op jit(solution)/shard_map/all_gather | solution.py:12
  190.9 102.2 %all-gather.17.cloned.1.call-start = ((), (), s32[]{:S(2)}) async-start(), calls=%async_computation.7 | async-start | bytes 2621440 | tf_op jit(solution)/shard_map/all_gather | solution.py:30
  223.8 110.4 %all-gather.21.cloned.1.call-start = ((), (), s32[]{:S(2)}) async-start(), calls=%async_computation.9 | async-start | bytes 5570560 | tf_op jit(solution)/shard_map/all_gather | solution.py:12
  224.6 161.2 %all-gather.23.cloned.1.call-start = ((), (), s32[]{:S(2)}) async-start(), calls=%async_computation.10 | async-start | bytes 5570560 | tf_op jit(solution)/shard_map/all_gather | solution.py:40
  225.3 202.7 %reduce-scatter.5.cloned.1.call-start = ((), (), s32[]{:S(2)}) async-start(), calls=%async_computation.11 | async-start | bytes 2621440 | tf_op jit(solution)/shard_map/reduce_scatter | solution.py:19
  293.1 92.7 %copy-start.7 = (bf16[512,2048]{1,0:T(8,128)(2,1)S(1)}, bf16[512,2048]{1,0:T(8,128)(2,1)}, u32[]{:S(2)}) copy-start(bf16[512,2048]{1,0:T(8,128)(2,1)} %all-gather.17.cloned.1.call-done) | copy-start | bytes 6291460
  398.3 30.9 %copy-start.5 = (f32[2048]{0:T(1024)S(1)}, f32[2048]{0:T(1024)}, u32[]{:S(2)}) copy-start(f32[2048]{0:T(1024)} %param.25) | copy-start | bytes 24580
Sparse Core Ops, SparseCore 0:
  9.9 34.0 all-gather.8
  45.7 39.3 all-gather.10
  86.8 39.4 all-gather.12
  127.8 49.9 all-gather.14
  190.4 29.4 reduce-scatter.2
  221.5 38.9 all-gather.18
  262.2 30.9 all-gather.16
  294.8 39.3 all-gather.20
  335.9 49.9 all-gather.22
  398.5 29.4 reduce-scatter.4
where the time goes:
time: 439 us; the launch traced here: 438 us
  waiting for transfers between devices  373 us (85%)
  matrix products  40.1 us (9%)
  between operations  13.6 us (3%)
  other arithmetic  10.7 us (2%)
    all_gather x4, waiting for transfers between devices, gathered(): return lax.all_gather(part, axis, axis=dim, tiled=True)  143 us
    all_gather x2, waiting for transfers between devices, half_branch(): down_block = lax.all_gather(down_piece, 'fs', axis=1, tiled=True)  103 us
    all_gather x2, waiting for transfers between devices, half_branch(): all_rows = lax.all_gather(normed, 'tp', axis=0, tiled=True)  64.7 us
    reduce_scatter x2, waiting for transfers between devices, own_rows(): lax.psum_scatter(everything.astype(jnp.bfloat16), axis, scatter_dimension...  58.1 us
    dot_general x2, matrix products, row_term(): return jnp.dot(rows, down_block, preferred_element_type=jnp.float32)  25 us
    dot_general x2, matrix products, add_rows(): gate_part = jnp.dot(columns, pieces[0], preferred_element_type=jnp.float32)  15.1 us
  transfers between devices with their start and end apart: 10, of which 10 were waited for; matrix products, arithmetic and copies ran while one was open for 4% of the time, Pallas kernels for 0%

commit v1 on v0

--- a/solution.py
+++ b/solution.py
@@ -37,7 +37,7 @@
         return (totals[0] + gate_part, totals[1] + value_part)
 
     gate_sum, value_sum = over_all((gate_piece, value_piece), "fs", 0, add_rows, (empty, empty))
-    down_block = lax.all_gather(down_piece, "fs", axis=1, tiled=True)
+    down_block = jnp.concatenate(lax.all_gather(down_piece, "fs"), axis=1)
     hidden = (jax.nn.silu(gate_sum) * value_sum).astype(jnp.bfloat16)
 
     def row_term(start, count):

time: 439 us -> 418 us (0.952)
  waiting for transfers between devices: 373 us -> 337 us
  local copies, waits for them, and re-layouts: 0.39 us -> 15.7 us
    all_gather x2, waiting for transfers between devices: 103 us -> 75.3 us  [half_branch(): down_block = jnp.concatenate(lax.all_gather(down_piece, 'fs'), axis=1)]
    reshape x0 -> x2, local copies, waits for them, and re-layouts: none -> 15.7 us  [half_branch(): down_block = jnp.concatenate(lax.all_gather(down_piece, 'fs'), axis=1)]
    all_gather x2, waiting for transfers between devices: 64.7 us -> 57.4 us  [half_branch(): all_rows = lax.all_gather(normed, 'tp', axis=0, tiled=True)]
  transfers between devices with their start and end apart: 10 -> 10, of which waited for: 10 -> 10; matrix products, arithmetic and copies ran while one was open for 4% -> 9% of each run, Pallas kernels for 0% -> 0%
where the time goes in v1:
time: 418 us; the launch traced here: 417 us
  waiting for transfers between devices  337 us (81%)
  matrix products  40.2 us (10%)
  local copies, waits for them, and re-layouts  15.7 us (4%)
  between operations  13.6 us (3%)
  other arithmetic  10.7 us (3%)
    all_gather x4, waiting for transfers between devices, gathered(): return lax.all_gather(part, axis, axis=dim, tiled=True)  141 us
    all_gather x2, waiting for transfers between devices, half_branch(): down_block = jnp.concatenate(lax.all_gather(down_piece, 'fs'), axis=1)  75.3 us
    reduce_scatter x2, waiting for transfers between devices, own_rows(): lax.psum_scatter(everything.astype(jnp.bfloat16), axis, scatter_dimension...  58.7 us
    all_gather x2, waiting for transfers between devices, half_branch(): all_rows = lax.all_gather(normed, 'tp', axis=0, tiled=True)  57.4 us
    dot_general x2, matrix products, row_term(): return jnp.dot(rows, down_block, preferred_element_type=jnp.float32)  24.9 us
    reshape x2, local copies, waits for them, and re-layouts, half_branch(): down_block = jnp.concatenate(lax.all_gather(down_piece, 'fs'), axis=1)  15.7 us
    dot_general x2, matrix products, add_rows(): gate_part = jnp.dot(columns, pieces[0], preferred_element_type=jnp.float32)  15.2 us
  transfers between devices with their start and end apart: 10, of which 10 were waited for; matrix products, arithmetic and copies ran while one was open for 9% of the time, Pallas kernels for 0%

profile of v1, /device:TPU:1, one launch (start us, length us, event | category | flops | bytes accessed | tf_op | source)
XLA Modules:
  0.0 417.4 jit_solution(10717617154942271827)
XLA Ops:
  6.5 0.7 all-gather.23.cloned.1.call-update
  7.3 1.2 fusion.12
  8.5 2.0 fusion.14
  12.0 39.6 %all-gather.23.cloned.1.call-done = bf16[20480,128]{1,0:T(8,128)(2,1)} async-done(((bf16[1280,128]{1,0:T(8,128)(2,1)}), bf16[20480,128]{1,0:T(8,128)(2,1)}) %all-gather.23.cloned.1.call-update) | async-done | bytes 5242896 | tf_op jit(solution)/shard_map/all_gather | solution.py:40
  51.6 7.9 %copy.14 = bf16[1280,16,128]{0,2,1:T(8,128)(2,1)} copy(bf16[1280,16,128]{2,0,1:T(8,128)(2,1)} %bitcast.19) | data formatting | bytes 10485760 | tf_op jit(solution)/shard_map/reshape | solution.py:40
  59.5 24.7 %all-gather.11.cloned.1.call-done = bf16[512,2048]{1,0:T(8,128)(2,1)} async-done(((bf16[128,2048]{1,0:T(8,128)(2,1)}), bf16[512,2048]{1,0:T(8,128)(2,1)}) %all-gather.11.cloned.1.call-update) | async-done | bytes 2097168 | tf_op jit(solution)/shard_map/all_gather | solution.py:30
  84.2 41.1 %all-gather.13.cloned.1.call-done = bf16[2048,1280]{1,0:T(8,128)(2,1)} async-done(((bf16[128,1280]{1,0:T(8,128)(2,1)}), bf16[2048,1280]{1,0:T(8,128)(2,1)}) %all-gather.13.cloned.1.call-update) | async-done | bytes 5242896 | tf_op jit(solution)/shard_map/all_gather | solution.py:12
  125.4 7.5 %fusion.22 = f32[512,1280]{1,0:T(8,128)} fusion(bf16[512,2048]{1,0:T(8,128)(2,1)} %all-gather.11.cloned.1.call-done, bf16[2048,1280]{1,0:T(8,128)(2,1)} %all-gather.13.cloned.1.call-done), kind=kOutput, calls=%fused_computation.42 | convolution fusion | flops 2684354560 | bytes 9961472 | tf_op jit(solution)/shard_map/dot_general | solution.py:35
  132.9 33.5 %all-gather.15.cloned.1.call-done = bf16[2048,1280]{1,0:T(8,128)(2,1)} async-done(((bf16[128,1280]{1,0:T(8,128)(2,1)}), bf16[2048,1280]{1,0:T(8,128)(2,1)}) %all-gather.15.cloned.1.call-update) | async-done | bytes 5242896 | tf_op jit(solution)/shard_map/all_gather | solution.py:12
  166.4 12.5 %convolution_convert_fusion.1 = bf16[512,2048]{1,0:T(8,128)(2,1)} fusion(bf16[1280,2048]{0,1:T(8,128)(2,1)} %bitcast.20, bf16[512,2048]{1,0:T(8,128)(2,1)S(1)} %copy-done.6, bf16[2048,1280]{1,0:T(8,128)(2,1)} %all-gather.15.cloned.1.call-done, f32[512,1280]{1,0:T(8,128)} %fusion.22), kind=kOutput, calls=%fused_computation.5 | convolution fusion | flops 5373689856 | bytes 17301504 | tf_op jit(solution)/shard_map/dot_general | solution.py:45
  180.5 28.5 %reduce-scatter.3.cloned.1.call-done = bf16[128,2048]{1,0:T(8,128)(2,1)} async-done(((bf16[512,2048]{1,0:T(8,128)(2,1)}), bf16[128,2048]{1,0:T(8,128)(2,1)}) %reduce-scatter.3.cloned.1.call-update) | async-done | bytes 524304 | tf_op jit(solution)/shard_map/reduce_scatter | solution.py:19
  209.1 1.2 fusion.2
  210.3 1.6 fusion.15
  212.0 1.0 fusion.17
  213.9 35.7 %all-gather.25.cloned.1.call-done = bf16[20480,128]{1,0:T(8,128)(2,1)} async-done(((bf16[1280,128]{1,0:T(8,128)(2,1)}), bf16[20480,128]{1,0:T(8,128)(2,1)}) %all-gather.25.cloned.1.call-update) | async-done | bytes 5242896 | tf_op jit(solution)/shard_map/all_gather | solution.py:40
  249.6 7.8 %copy.15 = bf16[1280,16,128]{0,2,1:T(8,128)(2,1)} copy(bf16[1280,16,128]{2,0,1:T(8,128)(2,1)} %bitcast.18) | data formatting | bytes 10485760 | tf_op jit(solution)/shard_map/reshape | solution.py:40
  257.4 33.4 %all-gather.19.cloned.1.call-done = bf16[2048,1280]{1,0:T(8,128)(2,1)} async-done(((bf16[128,1280]{1,0:T(8,128)(2,1)}), bf16[2048,1280]{1,0:T(8,128)(2,1)}) %all-gather.19.cloned.1.call-update) | async-done | bytes 5242896 | tf_op jit(solution)/shard_map/all_gather | solution.py:12
  290.8 32.6 %all-gather.17.cloned.1.call-done = bf16[512,2048]{1,0:T(8,128)(2,1)} async-done(((bf16[128,2048]{1,0:T(8,128)(2,1)}), bf16[512,2048]{1,0:T(8,128)(2,1)}) %all-gather.17.cloned.1.call-update) | async-done | bytes 2097168 | tf_op jit(solution)/shard_map/all_gather | solution.py:30
  323.5 7.7 %fusion.23 = f32[512,1280]{1,0:T(8,128)} fusion(bf16[512,2048]{1,0:T(8,128)(2,1)} %all-gather.17.cloned.1.call-done, bf16[2048,1280]{1,0:T(8,128)(2,1)} %all-gather.19.cloned.1.call-done), kind=kOutput, calls=%fused_computation.43 | convolution fusion | flops 2684354560 | bytes 9961472 | tf_op jit(solution)/shard_map/dot_general | solution.py:35
  331.2 33.4 %all-gather.21.cloned.1.call-done = bf16[2048,1280]{1,0:T(8,128)(2,1)} async-done(((bf16[128,1280]{1,0:T(8,128)(2,1)}), bf16[2048,1280]{1,0:T(8,128)(2,1)}) %all-gather.21.cloned.1.call-update) | async-done | bytes 5242896 | tf_op jit(solution)/shard_map/all_gather | solution.py:12
  364.6 12.5 %convolution_convert_fusion = bf16[512,2048]{1,0:T(8,128)(2,1)} fusion(bf16[1280,2048]{0,1:T(8,128)(2,1)} %bitcast.21, bf16[512,2048]{1,0:T(8,128)(2,1)S(1)} %copy-done.7, bf16[2048,1280]{1,0:T(8,128)(2,1)} %all-gather.21.cloned.1.call-done, f32[512,1280]{1,0:T(8,128)} %fusion.23), kind=kOutput, calls=%fused_computation.4 | convolution fusion | flops 5373689856 | bytes 17301504 | tf_op jit(solution)/shard_map/dot_general | solution.py:45
  377.1 30.1 %reduce-scatter.5.cloned.1.call-done = bf16[128,2048]{1,0:T(8,128)(2,1)} async-done(((bf16[512,2048]{1,0:T(8,128)(2,1)}), bf16[128,2048]{1,0:T(8,128)(2,1)}) %reduce-scatter.5.cloned.1.call-update) | async-done | bytes 524304 | tf_op jit(solution)/shard_map/reduce_scatter | solution.py:19
  407.2 1.2 fusion.9
  408.4 2.1 fusion.18
  (41 shorter events, 4.0 us)
Async XLA Ops:
  6.5 45.1 %all-gather.23.cloned.1.call-start = ((), (), s32[]{:S(2)}) async-start(), calls=%async_computation.10 | async-start | bytes 5570560 | tf_op jit(solution)/shard_map/all_gather | solution.py:40
  7.3 77.0 %all-gather.11.cloned.1.call-start = ((), (), s32[]{:S(2)}) async-start(), calls=%async_computation.2 | async-start | bytes 2621440 | tf_op jit(solution)/shard_map/all_gather | solution.py:30
  10.6 114.8 %all-gather.13.cloned.1.call-start = ((), (), s32[]{:S(2)}) async-start(), calls=%async_computation.3 | async-start | bytes 5570560 | tf_op jit(solution)/shard_map/all_gather | solution.py:12
  11.3 155.1 %all-gather.15.cloned.1.call-start = ((), (), s32[]{:S(2)}) async-start(), calls=%async_computation.4 | async-start | bytes 5570560 | tf_op jit(solution)/shard_map/all_gather | solution.py:12
  11.9 197.2 %reduce-scatter.3.cloned.1.call-start = ((), (), s32[]{:S(2)}) async-start(), calls=%async_computation.5 | async-start | bytes 2621440 | tf_op jit(solution)/shard_map/reduce_scatter | solution.py:19
  84.2 82.2 %copy-start.6 = (bf16[512,2048]{1,0:T(8,128)(2,1)S(1)}, bf16[512,2048]{1,0:T(8,128)(2,1)}, u32[]{:S(2)}) copy-start(bf16[512,2048]{1,0:T(8,128)(2,1)} %all-gather.11.cloned.1.call-done) | copy-start | bytes 6291460
  178.9 1.4 copy-start.1
  178.9 31.4 %copy-start = (bf16[128,2048]{1,0:T(8,128)(2,1)S(1)}, bf16[128,2048]{1,0:T(8,128)(2,1)}, u32[]{:S(2)}) copy-start(bf16[128,2048]{1,0:T(8,128)(2,1)} %param.13) | copy-start | bytes 1572868
  178.9 31.4 %copy-start.2 = (f32[2048]{0:T(1024)S(1)}, f32[2048]{0:T(1024)}, u32[]{:S(2)}) copy-start(f32[2048]{0:T(1024)} %param.20) | copy-start | bytes 24580
  178.9 31.4 %copy-start.3 = (f32[2048]{0:T(1024)S(1)}, f32[2048]{0:T(1024)}, u32[]{:S(2)}) copy-start(f32[2048]{0:T(1024)} %param.19) | copy-start | bytes 24580
  178.9 33.1 %copy-start.4 = (f32[2048]{0:T(1024)S(1)}, f32[2048]{0:T(1024)}, u32[]{:S(2)}) copy-start(f32[2048]{0:T(1024)} %param.21) | copy-start | bytes 24580
  178.9 70.7 %all-gather.25.cloned.1.call-start = ((), (), s32[]{:S(2)}) async-start(), calls=%async_computation.11 | async-start | bytes 5570560 | tf_op jit(solution)/shard_map/all_gather | solution.py:40
  179.5 111.3 %all-gather.19.cloned.1.call-start = ((), (), s32[]{:S(2)}) async-start(), calls=%async_computation.7 | async-start | bytes 5570560 | tf_op jit(solution)/shard_map/all_gather | solution.py:12
  180.3 143.2 %all-gather.17.cloned.1.call-start = ((), (), s32[]{:S(2)}) async-start(), calls=%async_computation.6 | async-start | bytes 2621440 | tf_op jit(solution)/shard_map/all_gather | solution.py:30
  213.0 151.6 %all-gather.21.cloned.1.call-start = ((), (), s32[]{:S(2)}) async-start(), calls=%async_computation.8 | async-start | bytes 5570560 | tf_op jit(solution)/shard_map/all_gather | solution.py:12
  213.7 193.5 %reduce-scatter.5.cloned.1.call-start = ((), (), s32[]{:S(2)}) async-start(), calls=%async_computation.9 | async-start | bytes 2621440 | tf_op jit(solution)/shard_map/reduce_scatter | solution.py:19
  323.5 41.1 %copy-start.7 = (bf16[512,2048]{1,0:T(8,128)(2,1)S(1)}, bf16[512,2048]{1,0:T(8,128)(2,1)}, u32[]{:S(2)}) copy-start(bf16[512,2048]{1,0:T(8,128)(2,1)} %all-gather.17.cloned.1.call-done) | copy-start | bytes 6291460
  377.1 31.4 %copy-start.5 = (f32[2048]{0:T(1024)S(1)}, f32[2048]{0:T(1024)}, u32[]{:S(2)}) copy-start(f32[2048]{0:T(1024)} %param.25) | copy-start | bytes 24580
Sparse Core Ops, SparseCore 0:
  9.0 42.5 all-gather.22
  53.3 30.9 all-gather.10
  86.0 39.3 all-gather.12
  126.9 39.4 all-gather.14
  179.1 29.9 reduce-scatter.2
  210.6 38.9 all-gather.24
  251.3 39.4 all-gather.18
  292.5 30.9 all-gather.16
  325.2 39.3 all-gather.20
  377.2 29.9 reduce-scatter.4
